TPU v7x, 32 devices: a whole 2x2x4 slice. The times are simulated.
32 devices in a mesh: sp: 8 (over z, y), tp: 4 (over x, core).
Axes of the slice: x: 2, y: 2, z: 4, core: 2. Of those that a mesh axis runs over, the one named last changes fastest.
Arguments:
- stream: bfloat16 [8192, 4096], P('sp', 'tp'), may hold values from -11 to 11
- norm_gain: bfloat16 [3, 4096], P(None, 'tp'), may hold values from 0.099609375 to 1.8984375
- pool_weight: bfloat16 [3, 4, 1024, 1024], P(None, 'tp', 'sp'), may hold values from -0.1875 to 0.1875
- pool_scale: bfloat16 [3, 4096], P(None, 'tp'), may hold values from 0.099609375 to 1.8984375
Outputs:
- mixed: bfloat16 [8192, 4096], P('sp', 'tp')
All inputs are finite; a program needn't handle non-finite values.
Results may differ from a plain program's by a relative error of at most 0.015.
Values may be sent and summed in bfloat16 or wider, within the bound.
A program may use at most 64 MiB of HBM per device.

v0:
```python
import jax
import jax.numpy as jnp
from jax import lax
from jax.sharding import PartitionSpec as P

D = 4096
POOL_GROUPS = 4
norm_eps = 1e-06


def padded(value, sides, width):
    for axis, dim in sides:
        devices, length = (lax.axis_size(axis), value.shape[dim])
        up = [(i, (i + 1) % devices) for i in range(devices - 1)]
        down = [(j, i) for i, j in up]
        last = lax.slice_in_dim(value, length - width, length, axis=dim)
        initial = lax.slice_in_dim(value, 0, width, axis=dim)
        before = lax.ppermute(last, axis, up)
        after = lax.ppermute(initial, axis, down)
        value = jnp.concatenate([before, value, after], axis=dim)
    return value


def window_pool(extended, out_rows, centre, halves, seq_total, reach_rows, per_dev, group_width):
    ext_float = extended.astype(jnp.float32).reshape(extended.shape[0], per_dev, group_width)
    window_sums = jnp.zeros((out_rows, per_dev, group_width), jnp.float32)
    for offset in range(-reach_rows, reach_rows):
        in_window = ((offset >= -halves) & (offset < halves)).astype(jnp.float32)
        window_sums = (
            window_sums
            + ext_float[reach_rows + offset : reach_rows + offset + out_rows]
            * in_window[None, :, None]
        )
    low_end = jnp.maximum(centre[:, None] - halves[None, :], 0)
    high_end = jnp.minimum(centre[:, None] + halves[None, :], seq_total)
    counts = jnp.maximum(high_end - low_end, 1).astype(jnp.float32)
    middle = ext_float[reach_rows : reach_rows + out_rows]
    return (window_sums / counts[:, :, None] - middle).astype(jnp.bfloat16)


def local(stream, norm_gain, pool_weight, pool_scale):
    tok_rows, local_width = stream.shape
    layers, per_dev, shard_rows, group_width = pool_weight.shape
    reach_rows = 2**POOL_GROUPS // 2
    seq_total = tok_rows * lax.axis_size("sp")
    first_pos = lax.axis_index("sp") * tok_rows
    groups = lax.axis_index("tp") * per_dev + jnp.arange(per_dev, dtype=jnp.int32)
    halves = jnp.left_shift(jnp.int32(1), groups)
    deep_rows = reach_rows * layers
    current = padded(stream, (("sp", 0),), deep_rows)
    base_pos = first_pos - deep_rows
    for layer_idx in range(layers):
        ext_rows = current.shape[0]
        positions = base_pos + jnp.arange(ext_rows, dtype=jnp.int32)
        inside = (positions >= 0) & (positions < seq_total)
        current_f = current.astype(jnp.float32)
        square_sums = lax.psum(jnp.sum(current_f * current_f, axis=1), "tp")
        row_scale = lax.rsqrt(square_sums / D + norm_eps)
        normed = current_f * row_scale[:, None] * norm_gain[layer_idx].astype(jnp.float32)
        normed = jnp.where(inside[:, None], normed, 0.0).astype(jnp.bfloat16)
        out_rows = ext_rows - 2 * reach_rows
        residual = current_f[reach_rows : ext_rows - reach_rows]
        centre = positions[reach_rows : ext_rows - reach_rows]
        base_pos = base_pos + reach_rows
        pooled = window_pool(
            normed, out_rows, centre, halves, seq_total, reach_rows, per_dev, group_width
        )
        branch = jnp.einsum(
            "tgc,gcd->tgd",
            pooled,
            lax.all_gather(pool_weight[layer_idx], "sp", axis=1, tiled=True),
            preferred_element_type=jnp.float32,
        )
        branch = branch.reshape(out_rows, local_width)
        current = (residual + branch * pool_scale[layer_idx].astype(jnp.float32)).astype(
            jnp.bfloat16
        )
    return current


def solution(mesh):
    placed = (P("sp", "tp"), P(None, "tp"), P(None, "tp", "sp", None), P(None, "tp"))
    return jax.shard_map(
        local, mesh=mesh, in_specs=placed, out_specs=P("sp", "tp"), check_vma=False
    )
```

profile of v0, /device:TPU:0, one launch (start us, length us, event | category | flops | bytes accessed | tf_op | source)
XLA Modules:
  0.0 213.5 jit_solution(14513719529926578591)
XLA Ops:
  6.5 0.0 copy-start
  6.5 0.0 all-gather.7.cloned.1.call-start
  6.5 2.2 %fusion.70 = (bf16[1,1,128,1024]{3,2,1,0:T(8,128)(2,1)}, bf16[1,1,128,1024]{3,2,1,0:T(8,128)(2,1)}, bf16[1,1,128,1024]{3,2,1,0:T(8,128)(2,1)}) fusion(bf16[3,1,128,1024]{3,2,1,0:T(8,128)(2,1)} %param.6), kind=kLoop, calls=%fused_computation.141 | loop fusion | bytes 1572864 | tf_op jit(solution)/shard_map/slice | solution.py:71
  8.7 0.0 all-gather.7.cloned.1.call-update
  8.7 0.0 all-gather.9.cloned.1.call-start
  8.8 0.7 all-gather.9.cloned.1.call-update
  9.5 0.0 all-gather.11.cloned.1.call-start
  9.5 0.8 fusion.69
  10.4 4.9 %collective-permute-start = (bf16[24,1024]{1,0:T(8,128)(2,1)S(1)}, bf16[24,1024]{1,0:T(8,128)(2,1)S(1)}, u32[]{:S(2)}, u32[]{:S(2)}) collective-permute-start(bf16[24,1024]{1,0:T(8,128)(2,1)S(1)} %get-tuple-element.5), channel_id=1, source_target_pairs={{0,4},{4,8},{8,12},{12,16},{16,20},{20,24},{24,28},{1,5},{5,9},{9,... | collective-permute-start | bytes 147464 | tf_op jit(solution)/shard_map/ppermute | solution.py:18
  15.3 1.3 collective-permute-start.1
  16.6 0.0 all-gather.11.cloned.1.call-update
  16.6 0.8 slice_convert_fusion.1
  17.5 0.8 slice_convert_fusion
  18.3 0.1 maximum_convert_fusion.2
  18.4 0.1 maximum_convert_fusion.1
  18.5 0.1 maximum_convert_fusion.3
  18.7 0.0 collective-permute-done
  18.7 2.5 %collective-permute-done.1 = bf16[24,1024]{1,0:T(8,128)(2,1)S(1)} collective-permute-done((bf16[24,1024]{1,0:T(8,128)(2,1)S(1)}, bf16[24,1024]{1,0:T(8,128)(2,1)S(1)}, u32[]{:S(2)}, u32[]{:S(2)}) %collective-permute-start.1) | collective-permute-done | bytes 49184 | tf_op jit(solution)/shard_map/ppermute | solution.py:19
  21.2 0.0 copy-done
  21.2 0.5 multiply_reduce_fusion
  21.8 6.2 %psum.21 = f32[1072]{0:T(1024)S(1)} all-reduce(f32[1072]{0:T(1024)S(1)} %multiply_reduce_fusion), channel_id=1, replica_groups=mesh['sp'=8,'tp'=4] {'tp'}, use_global_device_ids=true, to_apply=%region_1.0 | all-reduce | flops 1072 | bytes 8576 | tf_op jit(solution)/shard_map/psum | solution.py:57
  27.9 2.5 %maximum_convert_fusion = f32[1072,1024]{1,0:T(8,128)} fusion(bf16[24,1024]{1,0:T(8,128)(2,1)S(1)} %collective-permute-done.1, bf16[1024,1024]{1,0:T(8,128)(2,1)S(1)} %copy-done, bf16[24,1024]{1,0:T(8,128)(2,1)S(1)} %collective-permute-done), kind=kLoop, calls=%fused_computation.115 | loop fusion | flops 6586368 | bytes 6586368 | tf_op jit(solution)/shard_map/convert_element_type | solution.py:56
  30.5 2.9 %fusion.59 = f32[1072,1024]{1,0:T(8,128)} fusion(f32[1024]{0:T(1024)S(1)} %bitcast.21, f32[1072]{0:T(1024)S(1)} %add_rsqrt_fusion.2, pred[1072]{0:T(1024)(128)(4,1)S(1)} %compare_and_fusion.2, bf16[24,1024]{1,0:T(8,128)(2,1)S(1)} %collective-permute-done.1, bf16[1024,1024]{1,0:T(8,128)(2,1)S(1)} %copy-done, bf16[24,1024]{1,0:T(8,128)(2,1)S(1)} %collective-permute-done), kind=kLoop, calls=%fused_computation.114 | loop fusion | flops 12075008 | bytes 6595824 | tf_op jit(solution)/shard_map/convert_element_type | solution.py:25
  33.4 28.0 %all-gather.7.cloned.1.call-done = bf16[1,1,1024,1024]{3,2,1,0:T(8,128)(2,1)} async-done(((bf16[1,1,128,1024]{3,2,1,0:T(8,128)(2,1)}), bf16[1,1,1024,1024]{3,2,1,0:T(8,128)(2,1)}) %all-gather.7.cloned.1.call-update) | async-done | bytes 2097168 | tf_op jit(solution)/shard_map/all_gather | solution.py:71
  61.4 42.3 %multiply_reduce_fusion.1 = (f32[1056]{0:T(1024)S(1)}, f32[1056,1024]{1,0:T(8,128)}) fusion(f32[1024]{0:T(1024)S(1)} %bitcast.24, bf16[1,1,1024,1024]{3,2,1,0:T(8,128)(2,1)} %all-gather.7.cloned.1.call-done, f32[1072,1024]{1,0:T(8,128)} %fusion.59, f32[1056]{0:T(1024)S(1)} %maximum_convert_fusion.2, f32[]{:T(128)S(6)} %mul.631, f32[]{:T(128)S(6)} %mul.628, ...), kind=kOutput, calls=%fused_computation.40 | convolution fusion | flops 2257845248 | bytes 79966528 | tf_op jit(solution)/shard_map/tgc,gcd->tgd/dot_general | solution.py:68
  103.7 6.3 %psum.22 = f32[1056]{0:T(1024)S(1)} all-reduce(f32[1056]{0:T(1024)S(1)} %get-tuple-element.16), channel_id=1, replica_groups=mesh['sp'=8,'tp'=4] {'tp'}, use_global_device_ids=true, to_apply=%region_3.4 | all-reduce | flops 1056 | bytes 8448 | tf_op jit(solution)/shard_map/psum | solution.py:57
  110.0 4.7 %fusion.60 = f32[1056,1024]{1,0:T(8,128)} fusion(f32[1056,1024]{1,0:T(8,128)} %get-tuple-element.17, f32[1024]{0:T(1024)S(1)} %bitcast.20, f32[1056]{0:T(1024)S(1)} %add_rsqrt_fusion.1, pred[1056]{0:T(1024)(128)(4,1)S(1)} %compare_and_fusion.1), kind=kLoop, calls=%fused_computation.116 | loop fusion | flops 5406720 | bytes 8660128 | tf_op jit(solution)/shard_map/convert_element_type | solution.py:25
  114.8 0.0 all-gather.9.cloned.1.call-done
  114.8 41.7 %multiply_reduce_fusion.2 = (f32[1040]{0:T(1024)S(1)}, f32[1040,1024]{1,0:T(8,128)}) fusion(f32[1024]{0:T(1024)S(1)} %bitcast.23, bf16[1,1,1024,1024]{3,2,1,0:T(8,128)(2,1)} %all-gather.9.cloned.1.call-done, f32[1056,1024]{1,0:T(8,128)} %fusion.60, f32[1040]{0:T(1024)S(1)} %maximum_convert_fusion.1, f32[]{:T(128)S(6)} %mul.631, f32[]{:T(128)S(6)} %mul.628, ...), kind=kOutput, calls=%fused_computation.75 | convolution fusion | flops 2223635456 | bytes 78786752 | tf_op jit(solution)/shard_map/tgc,gcd->tgd/dot_general | solution.py:68
  156.4 6.7 %psum.23 = f32[1040]{0:T(1024)S(1)} all-reduce(f32[1040]{0:T(1024)S(1)} %get-tuple-element.18), channel_id=1, replica_groups=mesh['sp'=8,'tp'=4] {'tp'}, use_global_device_ids=true, to_apply=%region_5.6 | all-reduce | flops 1040 | bytes 8320 | tf_op jit(solution)/shard_map/psum | solution.py:57
  163.1 4.7 %fusion.63 = f32[1040,1024]{1,0:T(8,128)} fusion(f32[1040,1024]{1,0:T(8,128)} %get-tuple-element.19, f32[1024]{0:T(1024)S(1)} %bitcast.19, f32[1040]{0:T(1024)S(1)} %add_rsqrt_fusion, pred[1040]{0:T(1024)(128)(4,1)S(1)} %compare_and_fusion), kind=kLoop, calls=%fused_computation.118 | loop fusion | flops 5324800 | bytes 8528976 | tf_op jit(solution)/shard_map/convert_element_type | solution.py:25
  167.8 0.0 all-gather.11.cloned.1.call-done
  167.8 39.2 %fusion.55 = bf16[1024,1024]{1,0:T(8,128)(2,1)} fusion(f32[1040,1024]{1,0:T(8,128)} %get-tuple-element.19, bf16[1,1,1024,1024]{3,2,1,0:T(8,128)(2,1)} %all-gather.11.cloned.1.call-done, f32[1024]{0:T(1024)S(1)} %bitcast.22, f32[1040,1024]{1,0:T(8,128)} %fusion.63, f32[1024]{0:T(1024)S(1)} %maximum_convert_fusion.3, f32[]{:T(128)S(6)} %mul.631, ...), kind=kOutput, calls=%fused_computation.110 | convolution fusion | flops 2186280960 | bytes 75505728 | tf_op jit(solution)/shard_map/tgc,gcd->tgd/dot_general | solution.py:68
  (9 shorter events, 0.1 us)
Async XLA Ops:
  6.5 14.7 %copy-start = (bf16[1024,1024]{1,0:T(8,128)(2,1)S(1)}, bf16[1024,1024]{1,0:T(8,128)(2,1)}, u32[]{:S(2)}) copy-start(bf16[1024,1024]{1,0:T(8,128)(2,1)} %param.4) | copy-start | bytes 6291460
  6.5 54.9 %all-gather.7.cloned.1.call-start = ((), (), s32[]{:S(2)}) async-start(), calls=%async_computation | async-start | bytes 2359296 | tf_op jit(solution)/shard_map/all_gather | solution.py:71
  8.7 106.1 %all-gather.9.cloned.1.call-start = ((), (), s32[]{:S(2)}) async-start(), calls=%async_computation.1 | async-start | bytes 2359296 | tf_op jit(solution)/shard_map/all_gather | solution.py:71
  9.5 158.3 %all-gather.11.cloned.1.call-start = ((), (), s32[]{:S(2)}) async-start(), calls=%async_computation.2 | async-start | bytes 2359296 | tf_op jit(solution)/shard_map/all_gather | solution.py:71
  10.4 8.3 %collective-permute-start = (bf16[24,1024]{1,0:T(8,128)(2,1)S(1)}, bf16[24,1024]{1,0:T(8,128)(2,1)S(1)}, u32[]{:S(2)}, u32[]{:S(2)}) collective-permute-start(bf16[24,1024]{1,0:T(8,128)(2,1)S(1)} %get-tuple-element.5), channel_id=1, source_target_pairs={{0,4},{4,8},{8,12},{12,16},{16,20},{20,24},{24,28},{1,5},{5,9},{9,... | collective-permute-start | bytes 147464 | tf_op jit(solution)/shard_map/ppermute | solution.py:18
  15.3 6.0 %collective-permute-start.1 = (bf16[24,1024]{1,0:T(8,128)(2,1)S(1)}, bf16[24,1024]{1,0:T(8,128)(2,1)S(1)}, u32[]{:S(2)}, u32[]{:S(2)}) collective-permute-start(bf16[24,1024]{1,0:T(8,128)(2,1)S(1)} %get-tuple-element.6), channel_id=1, source_target_pairs={{4,0},{8,4},{12,8},{16,12},{20,16},{24,20},{28,24},{5,1},{9,5},{13... | collective-permute-start | bytes 147464 | tf_op jit(solution)/shard_map/ppermute | solution.py:19
Sparse Core Ops, SparseCore 0:
  9.5 51.8 all-gather.6
  63.5 47.6 all-gather.8
  113.3 47.6 all-gather.10
where the time goes:
time: 214 us
  matrix products  123 us (57%)
  waiting for transfers between devices  31.3 us (15%)
  blocking collectives  19.2 us (9%)
  other arithmetic  17.3 us (8%)
  between operations  13.4 us (6%)
  starting transfers between devices  6.26 us (3%)
  local copies, waits for them, and re-layouts  3 us (1%)
    dot_general x3, matrix products, local(): jnp.einsum('tgc,gcd->tgd', pooled, lax.all_gather(pool_weight[layer_idx],...  123 us
    all_gather x3, waiting for transfers between devices, local(): lax.all_gather(pool_weight[layer_idx], 'sp', axis=1, tiled=True)  28 us
    psum x3, blocking collectives, local(): square_sums = lax.psum(jnp.sum(current_f * current_f, axis=1), 'tp')  19.2 us
    convert_element_type x3, other arithmetic, window_pool(): extended.astype(jnp.float32)  12.3 us
    ppermute x1, starting transfers between devices, padded(): before = lax.ppermute(last, axis, up)  4.89 us
  transfers between devices with their start and end apart: 5, of which 2 were waited for; matrix products, arithmetic and copies ran while one was open for 48% of the time, Pallas kernels for 0%

commit v1 on v0

--- a/solution.py
+++ b/solution.py
@@ -6,6 +6,12 @@
 D = 4096
 POOL_GROUPS = 4
 norm_eps = 1e-06
+
+
+def all_parts(x, mesh_axis, along):
+    terms = lax.all_gather(x, mesh_axis, axis=0, tiled=False)
+    full = jnp.concatenate(terms, axis=along)
+    return full
 
 
 def padded(value, sides, width):
@@ -68,7 +74,7 @@
         branch = jnp.einsum(
             "tgc,gcd->tgd",
             pooled,
-            lax.all_gather(pool_weight[layer_idx], "sp", axis=1, tiled=True),
+            all_parts(pool_weight[layer_idx], "sp", 1),
             preferred_element_type=jnp.float32,
         )
         branch = branch.reshape(out_rows, local_width)

time: 214 us -> 214 us (level)
  no operation moved by 1% of the time
where the time goes in v1:
time: 214 us
  matrix products  123 us (57%)
  waiting for transfers between devices  31.3 us (15%)
  blocking collectives  19.2 us (9%)
  other arithmetic  17.3 us (8%)
  between operations  13.4 us (6%)
  starting transfers between devices  6.26 us (3%)
  local copies, waits for them, and re-layouts  3 us (1%)
    dot_general x3, matrix products, local(): jnp.einsum('tgc,gcd->tgd', pooled, all_parts(pool_weight[layer_idx], 'sp'...  123 us
    all_gather x3, waiting for transfers between devices, all_parts(): terms = lax.all_gather(x, mesh_axis, axis=0, tiled=False)  28 us
    psum x3, blocking collectives, local(): square_sums = lax.psum(jnp.sum(current_f * current_f, axis=1), 'tp')  19.2 us
    convert_element_type x3, other arithmetic, window_pool(): extended.astype(jnp.float32)  12.3 us
    ppermute x1, starting transfers between devices, padded(): before = lax.ppermute(last, axis, up)  4.89 us
  transfers between devices with their start and end apart: 5, of which 2 were waited for; matrix products, arithmetic and copies ran while one was open for 48% of the time, Pallas kernels for 0%

profile of v1, /device:TPU:0, one launch (start us, length us, event | category | flops | bytes accessed | tf_op | source)
XLA Modules:
  0.0 213.5 jit_solution(14513719529926578591)
XLA Ops:
  6.5 0.0 copy-start
  6.5 0.0 all-gather.4.cloned.1.call-start
  6.5 2.2 %fusion.67 = (bf16[1,1,128,1024]{3,2,1,0:T(8,128)(2,1)}, bf16[1,1,128,1024]{3,2,1,0:T(8,128)(2,1)}, bf16[1,1,128,1024]{3,2,1,0:T(8,128)(2,1)}) fusion(bf16[3,1,128,1024]{3,2,1,0:T(8,128)(2,1)} %param.6), kind=kLoop, calls=%fused_computation.138 | loop fusion | bytes 1572864 | tf_op jit(solution)/shard_map/slice | solution.py:77
  8.7 0.0 all-gather.4.cloned.1.call-update
  8.7 0.0 all-gather.6.cloned.1.call-start
  8.8 0.7 all-gather.6.cloned.1.call-update
  9.5 0.0 all-gather.8.cloned.1.call-start
  9.5 0.8 fusion.66
  10.4 4.9 %collective-permute-start = (bf16[24,1024]{1,0:T(8,128)(2,1)S(1)}, bf16[24,1024]{1,0:T(8,128)(2,1)S(1)}, u32[]{:S(2)}, u32[]{:S(2)}) collective-permute-start(bf16[24,1024]{1,0:T(8,128)(2,1)S(1)} %get-tuple-element.5), channel_id=1, source_target_pairs={{0,4},{4,8},{8,12},{12,16},{16,20},{20,24},{24,28},{1,5},{5,9},{9,... | collective-permute-start | bytes 147464 | tf_op jit(solution)/shard_map/ppermute | solution.py:24
  15.3 1.3 collective-permute-start.1
  16.6 0.0 all-gather.8.cloned.1.call-update
  16.6 0.8 slice_convert_fusion.1
  17.5 0.8 slice_convert_fusion
  18.3 0.1 maximum_convert_fusion.2
  18.4 0.1 maximum_convert_fusion.1
  18.5 0.1 maximum_convert_fusion.3
  18.7 0.0 collective-permute-done
  18.7 2.5 %collective-permute-done.1 = bf16[24,1024]{1,0:T(8,128)(2,1)S(1)} collective-permute-done((bf16[24,1024]{1,0:T(8,128)(2,1)S(1)}, bf16[24,1024]{1,0:T(8,128)(2,1)S(1)}, u32[]{:S(2)}, u32[]{:S(2)}) %collective-permute-start.1) | collective-permute-done | bytes 49184 | tf_op jit(solution)/shard_map/ppermute | solution.py:25
  21.2 0.0 copy-done
  21.2 0.5 multiply_reduce_fusion
  21.8 6.2 %psum.21 = f32[1072]{0:T(1024)S(1)} all-reduce(f32[1072]{0:T(1024)S(1)} %multiply_reduce_fusion), channel_id=1, replica_groups=mesh['sp'=8,'tp'=4] {'tp'}, use_global_device_ids=true, to_apply=%region_1.0 | all-reduce | flops 1072 | bytes 8576 | tf_op jit(solution)/shard_map/psum | solution.py:63
  27.9 2.5 %maximum_convert_fusion = f32[1072,1024]{1,0:T(8,128)} fusion(bf16[24,1024]{1,0:T(8,128)(2,1)S(1)} %collective-permute-done.1, bf16[1024,1024]{1,0:T(8,128)(2,1)S(1)} %copy-done, bf16[24,1024]{1,0:T(8,128)(2,1)S(1)} %collective-permute-done), kind=kLoop, calls=%fused_computation.115 | loop fusion | flops 6586368 | bytes 6586368 | tf_op jit(solution)/shard_map/convert_element_type | solution.py:62
  30.5 2.9 %fusion.59 = f32[1072,1024]{1,0:T(8,128)} fusion(f32[1024]{0:T(1024)S(1)} %bitcast.14, f32[1072]{0:T(1024)S(1)} %add_rsqrt_fusion.2, pred[1072]{0:T(1024)(128)(4,1)S(1)} %compare_and_fusion.2, bf16[24,1024]{1,0:T(8,128)(2,1)S(1)} %collective-permute-done.1, bf16[1024,1024]{1,0:T(8,128)(2,1)S(1)} %copy-done, bf16[24,1024]{1,0:T(8,128)(2,1)S(1)} %collective-permute-done), kind=kLoop, calls=%fused_computation.114 | loop fusion | flops 12075008 | bytes 6595824 | tf_op jit(solution)/shard_map/convert_element_type | solution.py:31
  33.4 28.0 %all-gather.4.cloned.1.call-done = bf16[8,1,128,1024]{3,2,1,0:T(8,128)(2,1)} async-done(((bf16[1,1,128,1024]{3,2,1,0:T(8,128)(2,1)}), bf16[8,1,128,1024]{3,2,1,0:T(8,128)(2,1)}) %all-gather.4.cloned.1.call-update) | async-done | bytes 2097168 | tf_op jit(solution)/shard_map/all_gather | solution.py:12
  61.4 42.3 %multiply_reduce_fusion.1 = (f32[1056]{0:T(1024)S(1)}, f32[1056,1024]{1,0:T(8,128)}) fusion(f32[1024]{0:T(1024)S(1)} %bitcast.17, bf16[1024,1024]{1,0:T(8,128)(2,1)} %bitcast.20, f32[1072,1024]{1,0:T(8,128)} %fusion.59, f32[1056]{0:T(1024)S(1)} %maximum_convert_fusion.2, f32[]{:T(128)S(6)} %mul.631, f32[]{:T(128)S(6)} %mul.628, f32[]{:T(128)S(6)} %mul.625, ...), kind=kOutput, calls=%fused_computation.40 | convolution fusion | flops 2257845248 | bytes 79966528 | tf_op jit(solution)/shard_map/tgc,gcd->tgd/dot_general | solution.py:74
  103.7 6.3 %psum.22 = f32[1056]{0:T(1024)S(1)} all-reduce(f32[1056]{0:T(1024)S(1)} %get-tuple-element.16), channel_id=1, replica_groups=mesh['sp'=8,'tp'=4] {'tp'}, use_global_device_ids=true, to_apply=%region_3.4 | all-reduce | flops 1056 | bytes 8448 | tf_op jit(solution)/shard_map/psum | solution.py:63
  110.0 4.7 %fusion.60 = f32[1056,1024]{1,0:T(8,128)} fusion(f32[1056,1024]{1,0:T(8,128)} %get-tuple-element.17, f32[1024]{0:T(1024)S(1)} %bitcast.13, f32[1056]{0:T(1024)S(1)} %add_rsqrt_fusion.1, pred[1056]{0:T(1024)(128)(4,1)S(1)} %compare_and_fusion.1), kind=kLoop, calls=%fused_computation.116 | loop fusion | flops 5406720 | bytes 8660128 | tf_op jit(solution)/shard_map/convert_element_type | solution.py:31
  114.8 0.0 all-gather.6.cloned.1.call-done
  114.8 41.7 %multiply_reduce_fusion.2 = (f32[1040]{0:T(1024)S(1)}, f32[1040,1024]{1,0:T(8,128)}) fusion(f32[1024]{0:T(1024)S(1)} %bitcast.16, bf16[1024,1024]{1,0:T(8,128)(2,1)} %bitcast.18, f32[1056,1024]{1,0:T(8,128)} %fusion.60, f32[1040]{0:T(1024)S(1)} %maximum_convert_fusion.1, f32[]{:T(128)S(6)} %mul.631, f32[]{:T(128)S(6)} %mul.628, f32[]{:T(128)S(6)} %mul.625, ...), kind=kOutput, calls=%fused_computation.75 | convolution fusion | flops 2223635456 | bytes 78786752 | tf_op jit(solution)/shard_map/tgc,gcd->tgd/dot_general | solution.py:74
  156.4 6.7 %psum.23 = f32[1040]{0:T(1024)S(1)} all-reduce(f32[1040]{0:T(1024)S(1)} %get-tuple-element.18), channel_id=1, replica_groups=mesh['sp'=8,'tp'=4] {'tp'}, use_global_device_ids=true, to_apply=%region_5.6 | all-reduce | flops 1040 | bytes 8320 | tf_op jit(solution)/shard_map/psum | solution.py:63
  163.1 4.7 %fusion.63 = f32[1040,1024]{1,0:T(8,128)} fusion(f32[1040,1024]{1,0:T(8,128)} %get-tuple-element.19, f32[1024]{0:T(1024)S(1)} %bitcast.12, f32[1040]{0:T(1024)S(1)} %add_rsqrt_fusion, pred[1040]{0:T(1024)(128)(4,1)S(1)} %compare_and_fusion), kind=kLoop, calls=%fused_computation.118 | loop fusion | flops 5324800 | bytes 8528976 | tf_op jit(solution)/shard_map/convert_element_type | solution.py:31
  167.8 0.0 all-gather.8.cloned.1.call-done
  167.8 39.2 %fusion.55 = bf16[1024,1024]{1,0:T(8,128)(2,1)} fusion(f32[1040,1024]{1,0:T(8,128)} %get-tuple-element.19, bf16[1024,1024]{1,0:T(8,128)(2,1)} %bitcast.19, f32[1024]{0:T(1024)S(1)} %bitcast.15, f32[1040,1024]{1,0:T(8,128)} %fusion.63, f32[1024]{0:T(1024)S(1)} %maximum_convert_fusion.3, f32[]{:T(128)S(6)} %mul.631, f32[]{:T(128)S(6)} %mul.628, ...), kind=kOutput, calls=%fused_computation.110 | convolution fusion | flops 2186280960 | bytes 75505728 | tf_op jit(solution)/shard_map/tgc,gcd->tgd/dot_general | solution.py:74
  (9 shorter events, 0.1 us)
Async XLA Ops:
  6.5 14.7 %copy-start = (bf16[1024,1024]{1,0:T(8,128)(2,1)S(1)}, bf16[1024,1024]{1,0:T(8,128)(2,1)}, u32[]{:S(2)}) copy-start(bf16[1024,1024]{1,0:T(8,128)(2,1)} %param.4) | copy-start | bytes 6291460
  6.5 54.9 %all-gather.4.cloned.1.call-start = ((), (), s32[]{:S(2)}) async-start(), calls=%async_computation | async-start | bytes 2359296 | tf_op jit(solution)/shard_map/all_gather | solution.py:12
  8.7 106.1 %all-gather.6.cloned.1.call-start = ((), (), s32[]{:S(2)}) async-start(), calls=%async_computation.1 | async-start | bytes 2359296 | tf_op jit(solution)/shard_map/all_gather | solution.py:12
  9.5 158.3 %all-gather.8.cloned.1.call-start = ((), (), s32[]{:S(2)}) async-start(), calls=%async_computation.2 | async-start | bytes 2359296 | tf_op jit(solution)/shard_map/all_gather | solution.py:12
  10.4 8.3 %collective-permute-start = (bf16[24,1024]{1,0:T(8,128)(2,1)S(1)}, bf16[24,1024]{1,0:T(8,128)(2,1)S(1)}, u32[]{:S(2)}, u32[]{:S(2)}) collective-permute-start(bf16[24,1024]{1,0:T(8,128)(2,1)S(1)} %get-tuple-element.5), channel_id=1, source_target_pairs={{0,4},{4,8},{8,12},{12,16},{16,20},{20,24},{24,28},{1,5},{5,9},{9,... | collective-permute-start | bytes 147464 | tf_op jit(solution)/shard_map/ppermute | solution.py:24
  15.3 6.0 %collective-permute-start.1 = (bf16[24,1024]{1,0:T(8,128)(2,1)S(1)}, bf16[24,1024]{1,0:T(8,128)(2,1)S(1)}, u32[]{:S(2)}, u32[]{:S(2)}) collective-permute-start(bf16[24,1024]{1,0:T(8,128)(2,1)S(1)} %get-tuple-element.6), channel_id=1, source_target_pairs={{4,0},{8,4},{12,8},{16,12},{20,16},{24,20},{28,24},{5,1},{9,5},{13... | collective-permute-start | bytes 147464 | tf_op jit(solution)/shard_map/ppermute | solution.py:25
Sparse Core Ops, SparseCore 0:
  9.5 51.8 all-gather.3
  63.5 47.6 all-gather.5
  113.3 47.6 all-gather.7
